TPU v7x, 32 devices: a whole 2x2x4 slice. The times are simulated.
32 devices in a mesh: fs: 8 (over z, x), tp: 4 (over y, core).
Axes of the slice: x: 2, y: 2, z: 4, core: 2. Of those that a mesh axis runs over, the one named last changes fastest.
Arguments:
- tokens: bfloat16 [320, 4096], P('fs'), may hold values from -6 to 6
- routes: int32 [320, 2], P('fs'), may hold values from 0 to 3, all different within a row; in each aligned block of 40 rows (0 to 39, 40 to 79, ...) at most 30 rows name the same one
- route_logits: float32 [320, 2], P('fs'), may hold values from -6 to 6
- norm_gain: float32 [4096], P('fs'), may hold values from 0.1 to 1.9
- gate_weight: float32 [4, 4096, 8192], P(None, 'fs', 'tp'), may hold values from -0.09375 to 0.09375
- up_weight: float32 [4, 4096, 8192], P(None, 'fs', 'tp'), may hold values from -0.09375 to 0.09375
- down_weight: float32 [4, 4096, 8192], P(None, 'fs', 'tp'), may hold values from -0.0625 to 0.0625
Outputs:
- mixed: bfloat16 [320, 4096], P('fs', 'tp')
- gate_sampler: bfloat16 [4, 4096, 8192], P('tp', None, 'fs')
- up_sampler: bfloat16 [4, 4096, 8192], P('tp', None, 'fs')
- down_sampler: bfloat16 [4, 4096, 8192], P('tp', None, 'fs')
Inputs may be any that keep to these rules, and one draw needn't show every extreme that they name: `routes`: the 2 experts of a token differ. Within the tokens of one index of fs (aligned blocks of 40 rows) no expert is named by more than 30 tokens.
All inputs are finite; a program needn't handle non-finite values.
Results may differ from a plain program's by a relative error of at most 0.01.
Values may be sent and summed in bfloat16 or wider, within the bound.
A program may use at most 192 MiB of HBM per device.

v0:
```python
import jax
import jax.numpy as jnp
from jax import lax
from jax.sharding import PartitionSpec as P

CAP = 30


def arrange(matrix, spread):
    experts, width, columns = matrix.shape
    block = columns // spread
    split = matrix.reshape(experts, width, spread, block)
    return jnp.transpose(split, (0, 2, 1, 3)).reshape(experts * spread, width, block)


def outgoing_rows(placing, row_data, experts, spread):
    packed = jnp.einsum(
        "rec,rd->ecd", placing.astype(jnp.bfloat16), row_data, preferred_element_type=jnp.float32
    ).astype(jnp.bfloat16)
    copies = jnp.broadcast_to(packed[:, None], (experts, spread) + packed.shape[1:])
    return copies.reshape((experts * spread,) + packed.shape[1:])


def per_device(tokens, routes, route_logits, norm_gain, gate_weight, up_weight, down_weight):
    experts = gate_weight.shape[0]
    fs_count = lax.axis_size("fs")
    spread = fs_count // experts
    gain_cols = norm_gain[None, :, None]
    gate_pieces = arrange((gate_weight * gain_cols).astype(jnp.bfloat16), spread)
    up_pieces = arrange((up_weight * gain_cols).astype(jnp.bfloat16), spread)
    down_pieces = arrange(down_weight.astype(jnp.bfloat16), spread)
    gate_local, up_local, down_local = (
        lax.all_to_all(gate_pieces, "fs", split_axis=0, concat_axis=1, tiled=True),
        lax.all_to_all(up_pieces, "fs", split_axis=0, concat_axis=1, tiled=True),
        lax.all_to_all(down_pieces, "fs", split_axis=0, concat_axis=1, tiled=True),
    )
    gate_matrix = gate_local[0]
    up_matrix = up_local[0]
    down_matrix = down_local[0]
    tok_float = tokens.astype(jnp.float32)
    normed = (
        tok_float * lax.rsqrt(jnp.mean(tok_float * tok_float, axis=1, keepdims=True) + 1e-05)
    ).astype(jnp.bfloat16)
    shares = jax.nn.sigmoid(route_logits - route_logits[:, ::-1])
    expert_ids = lax.broadcasted_iota(jnp.int32, (1, 1, experts), 2)
    picks = (routes[:, :, None] == expert_ids).astype(jnp.int32)
    member = jnp.sum(picks, axis=1)
    position = jnp.cumsum(member, axis=0) - member
    slot_ids = lax.broadcasted_iota(jnp.int32, (1, 1, CAP), 2)
    placing = ((position[:, :, None] == slot_ids) & (member[:, :, None] > 0)).astype(jnp.float32)
    weights = jnp.sum(picks.astype(jnp.float32) * shares[:, :, None], axis=1)
    combine = jnp.transpose(placing * weights[:, :, None], (1, 2, 0))
    cols_out = gate_matrix.shape[1]
    part_width = normed.shape[1] // lax.axis_size("tp")
    own_cols = lax.dynamic_slice_in_dim(normed, lax.axis_index("tp") * part_width, part_width, 1)
    sending = outgoing_rows(placing, own_cols, experts, spread)
    arrived = lax.all_to_all(sending, "fs", split_axis=0, concat_axis=0, tiled=True)
    segment = lax.all_gather(arrived, "tp", axis=2, tiled=True)
    flat_rows = segment.reshape(-1, segment.shape[2])
    gate_act = jnp.dot(flat_rows, gate_matrix, preferred_element_type=jnp.float32)
    up_act = jnp.dot(flat_rows, up_matrix, preferred_element_type=jnp.float32)
    hidden = (
        (jax.nn.silu(gate_act) * up_act)
        .astype(jnp.bfloat16)
        .reshape(arrived.shape[0], arrived.shape[1], cols_out)
    )
    slot_rows = hidden.reshape(-1, cols_out)
    summed = lax.psum_scatter(
        lax.dot_general(
            down_matrix, slot_rows, (((1,), (1,)), ((), ())), preferred_element_type=jnp.float32
        ),
        "tp",
        scatter_dimension=0,
        tiled=True,
    )
    back = lax.all_to_all(
        summed.reshape(summed.shape[0], fs_count, CAP),
        "fs",
        split_axis=1,
        concat_axis=1,
        tiled=True,
    )
    per_expert = jnp.sum(back.reshape(back.shape[0], experts, spread, CAP), axis=2)
    mixed = jnp.einsum("dec,ecr->rd", per_expert, combine, precision=lax.Precision.HIGHEST).astype(
        jnp.bfloat16
    )
    return (mixed, gate_local, up_local, down_local)


def solution(mesh):
    in_specs = (
        P("fs", None),
        P("fs", None),
        P("fs", None),
        P("fs"),
        P(None, "fs", "tp"),
        P(None, "fs", "tp"),
        P(None, "fs", "tp"),
    )
    out_specs = (P("fs", "tp"), P("tp", None, "fs"), P("tp", None, "fs"), P("tp", None, "fs"))
    return jax.shard_map(
        per_device, mesh=mesh, in_specs=in_specs, out_specs=out_specs, check_vma=False
    )
```

profile of v0, /device:TPU:0, one launch (start us, length us, event | category | flops | bytes accessed | tf_op | source)
XLA Modules:
  0.0 727.2 jit_solution(11316737366031616278)
XLA Ops:
  7.2 0.7 convert_reduce_fusion
  7.9 0.1 copy.23
  8.0 1.0 convert_element_type.41
  9.0 1.1 multiply_reduce_fusion
  10.1 0.1 reduce_window_sum.11
  10.2 0.1 copy.26
  10.3 0.3 convolution_convert_fusion
  10.6 0.9 broadcast_in_dim.2
  11.4 7.3 %all-to-all-start.1 = ((bf16[8,30,1024]{2,1,0:T(8,128)(2,1)}), bf16[8,30,1024]{2,1,0:T(8,128)(2,1)S(1)}, u32[]{:S(2)}, u32[]{:S(2)}) async-start(bf16[8,30,1024]{2,1,0:T(8,128)(2,1)} %bitcast.6), calls=%async_computation.1 | async-start | bytes 1048576 | tf_op jit(solution)/shard_map/all_to_all | solution.py:57
  18.7 11.9 %multiply_convert_fusion.1 = (bf16[4,512,2048]{2,1,0:T(8,128)(2,1)S(1)}, bf16[4,512,2048]{2,1,0:T(8,128)(2,1)S(1)}) fusion(f32[4,512,2048]{2,1,0:T(8,128)} %param.11, f32[512]{0:T(512)} %param.10, f32[4,512,2048]{2,1,0:T(8,128)} %param.12), kind=kLoop, calls=%fused_computation.1 | loop fusion | flops 16777216 | bytes 50333696 | tf_op jit(solution)/shard_map/convert_element_type | solution.py:29
  30.6 6.1 fusion.20
  36.7 7.8 %pad_maximum_fusion.1 = bf16[4,1024,1024]{2,1,0:T(8,128)(2,1)} fusion(bf16[4,512,1024]{2,1,0:T(8,128)(2,1)} %get-tuple-element.5, bf16[4,512,1024]{2,1,0:T(8,128)(2,1)} %get-tuple-element.4), kind=kLoop, calls=%fused_computation.3 | loop fusion | flops 16777216 | bytes 16777216 | tf_op jit(solution)/shard_map/concatenate.1
  44.6 0.0 all-to-all-done.1
  44.6 0.0 copy-start
  44.6 0.8 copy-done
  45.4 6.0 all-to-all-start.2
  51.4 7.8 %pad_maximum_fusion.2 = bf16[4,1024,1024]{2,1,0:T(8,128)(2,1)} fusion(bf16[4,512,1024]{2,1,0:T(8,128)(2,1)} %get-tuple-element.12, bf16[4,512,1024]{2,1,0:T(8,128)(2,1)} %get-tuple-element.13), kind=kLoop, calls=%fused_computation.4 | loop fusion | flops 16777216 | bytes 16777216 | tf_op jit(solution)/shard_map/concatenate.2
  59.2 174.8 %all-to-all-done.2 = bf16[8,512,1024]{2,1,0:T(8,128)(2,1)} async-done(((bf16[8,512,1024]{2,1,0:T(8,128)(2,1)}), bf16[8,512,1024]{2,1,0:T(8,128)(2,1)}, u32[]{:S(2)}, u32[]{:S(2)}) %all-to-all-start.2) | async-done | bytes 8388640 | tf_op jit(solution)/shard_map/all_to_all | solution.py:33
  234.0 5.0 all-to-all-start.3
  239.0 6.6 convert_element_type.38
  245.6 3.8 fusion.22
  249.4 7.8 %pad_maximum_fusion = bf16[4,1024,1024]{2,1,0:T(8,128)(2,1)} fusion(bf16[4,512,1024]{2,1,0:T(8,128)(2,1)} %get-tuple-element.9, bf16[4,512,1024]{2,1,0:T(8,128)(2,1)} %get-tuple-element.8), kind=kLoop, calls=%fused_computation.2 | loop fusion | flops 16777216 | bytes 16777216 | tf_op jit(solution)/shard_map/concatenate
  257.2 163.7 %all-to-all-done.3 = bf16[8,512,1024]{2,1,0:T(8,128)(2,1)} async-done(((bf16[8,512,1024]{2,1,0:T(8,128)(2,1)}), bf16[8,512,1024]{2,1,0:T(8,128)(2,1)}, u32[]{:S(2)}, u32[]{:S(2)}) %all-to-all-start.3) | async-done | bytes 8388640 | tf_op jit(solution)/shard_map/all_to_all | solution.py:34
  421.0 4.9 all-to-all-start
  425.9 0.0 all-gather.2.cloned.1.call-start
  426.0 0.7 all-gather.2.cloned.1.call-update
  426.6 0.2 reduce-scatter.2.cloned.1.call-start
  426.9 25.3 %all-gather.2.cloned.1.call-done = bf16[8,30,4096]{2,1,0:T(8,128)(2,1)} async-done(((bf16[8,30,1024]{2,1,0:T(8,128)(2,1)}), bf16[8,30,4096]{2,1,0:T(8,128)(2,1)}) %all-gather.2.cloned.1.call-update) | async-done | bytes 1966096 | tf_op jit(solution)/shard_map/all_gather | solution.py:58
  452.2 1.8 reshape.75
  454.1 5.6 fusion.23
  459.6 148.4 %all-to-all-done = bf16[8,512,1024]{2,1,0:T(8,128)(2,1)} async-done(((bf16[8,512,1024]{2,1,0:T(8,128)(2,1)}), bf16[8,512,1024]{2,1,0:T(8,128)(2,1)}, u32[]{:S(2)}, u32[]{:S(2)}) %all-to-all-start) | async-done | bytes 8388640 | tf_op jit(solution)/shard_map/all_to_all | solution.py:35
  608.1 0.0 copy-start.1
  608.1 0.0 copy-start.2
  608.1 12.2 %fusion.24 = f32[4096,240]{0,1:T(8,128)} fusion(bf16[4096,1024]{1,0:T(8,128)(2,1)} %bitcast.4, bf16[240,4096]{1,0:T(8,128)(2,1)S(1)} %reshape.75, bf16[4096,1024]{1,0:T(8,128)(2,1)} %bitcast.10, f32[240,1024]{1,0:T(8,128)S(1)} %fusion.23), kind=kOutput, calls=%fused_computation.42 | convolution fusion | flops 4028006400 | bytes 23658496 | tf_op jit(solution)/shard_map/dot_general | solution.py:69
  620.3 0.0 reduce-scatter.2.cloned.1.call-update
  620.3 42.2 %reduce-scatter.2.cloned.1.call-done = f32[1024,240]{0,1:T(8,128)} async-done(((f32[4096,240]{0,1:T(8,128)}), f32[1024,240]{0,1:T(8,128)}) %reduce-scatter.2.cloned.1.call-update) | async-done | bytes 983056 | tf_op jit(solution)/shard_map/reduce_scatter | solution.py:68
  662.5 2.3 reshape.78
  664.8 5.5 all-to-all-start.4
  670.3 0.1 copy.25
  670.4 0.0 copy-done.1
  670.4 0.0 copy-done.2
  670.5 25.5 %all-to-all-done.4 = f32[1024,8,30]{0,2,1:T(8,128)S(1)} async-done(((f32[1024,8,30]{0,2,1:T(8,128)}), f32[1024,8,30]{0,2,1:T(8,128)S(1)}, u32[]{:S(2)}, u32[]{:S(2)}) %all-to-all-start.4) | async-done | bytes 983072 | tf_op jit(solution)/shard_map/all_to_all | solution.py:76
  696.0 0.1 bitcast_reduce_fusion
  696.0 1.0 fusion.1
  697.1 7.8 %copy.30 = bf16[1,4096,1024]{2,1,0:T(8,128)(2,1)} copy(bf16[1,4096,1024]{2,1,0:T(8,128)(2,1)} %bitcast.13) | data formatting | bytes 16777216
  704.8 7.8 %copy.31 = bf16[1,4096,1024]{2,1,0:T(8,128)(2,1)} copy(bf16[1,4096,1024]{2,1,0:T(8,128)(2,1)} %bitcast.14) | data formatting | bytes 16777216
  712.6 7.8 %copy.32 = bf16[1,4096,1024]{2,1,0:T(8,128)(2,1)} copy(bf16[1,4096,1024]{2,1,0:T(8,128)(2,1)} %bitcast.15) | data formatting | bytes 16777216
  (7 shorter events, 0.1 us)
Async XLA Ops:
  11.4 33.1 %all-to-all-start.1 = ((bf16[8,30,1024]{2,1,0:T(8,128)(2,1)}), bf16[8,30,1024]{2,1,0:T(8,128)(2,1)S(1)}, u32[]{:S(2)}, u32[]{:S(2)}) async-start(bf16[8,30,1024]{2,1,0:T(8,128)(2,1)} %bitcast.6), calls=%async_computation.1 | async-start | bytes 1048576 | tf_op jit(solution)/shard_map/all_to_all | solution.py:57
  44.6 0.8 copy-start
  45.4 188.6 %all-to-all-start.2 = ((bf16[8,512,1024]{2,1,0:T(8,128)(2,1)}), bf16[8,512,1024]{2,1,0:T(8,128)(2,1)}, u32[]{:S(2)}, u32[]{:S(2)}) async-start(bf16[8,512,1024]{2,1,0:T(8,128)(2,1)} %bitcast.42), calls=%async_computation.2 | async-start | bytes 16777216 | tf_op jit(solution)/shard_map/all_to_all | solution.py:33
  234.0 187.0 %all-to-all-start.3 = ((bf16[8,512,1024]{2,1,0:T(8,128)(2,1)}), bf16[8,512,1024]{2,1,0:T(8,128)(2,1)}, u32[]{:S(2)}, u32[]{:S(2)}) async-start(bf16[8,512,1024]{2,1,0:T(8,128)(2,1)} %bitcast.41), calls=%async_computation.3 | async-start | bytes 16777216 | tf_op jit(solution)/shard_map/all_to_all | solution.py:34
  421.0 187.1 %all-to-all-start = ((bf16[8,512,1024]{2,1,0:T(8,128)(2,1)}), bf16[8,512,1024]{2,1,0:T(8,128)(2,1)}, u32[]{:S(2)}, u32[]{:S(2)}) async-start(bf16[8,512,1024]{2,1,0:T(8,128)(2,1)} %bitcast.40), calls=%async_computation | async-start | bytes 16777216 | tf_op jit(solution)/shard_map/all_to_all | solution.py:35
  425.9 26.3 %all-gather.2.cloned.1.call-start = ((), (), s32[]{:S(2)}) async-start(), calls=%async_computation.6 | async-start | bytes 2621440 | tf_op jit(solution)/shard_map/all_gather | solution.py:58
  426.6 235.9 %reduce-scatter.2.cloned.1.call-start = ((), (), s32[]{:S(2)}) async-start(), calls=%async_computation.7 | async-start | bytes 4915200 | tf_op jit(solution)/shard_map/reduce_scatter | solution.py:68
  608.1 62.3 %copy-start.1 = (f32[40,2]{0,1:T(2,128)S(1)}, f32[40,2]{0,1:T(2,128)}, u32[]{:S(2)}) copy-start(f32[40,2]{0,1:T(2,128)} %param.9) | copy-start | bytes 964
  608.1 62.4 %copy-start.2 = (s32[40,2]{0,1:T(2,128)S(1)}, s32[40,2]{0,1:T(2,128)}, u32[]{:S(2)}) copy-start(s32[40,2]{0,1:T(2,128)} %param.8) | copy-start | bytes 964
  664.8 31.2 %all-to-all-start.4 = ((f32[1024,8,30]{0,2,1:T(8,128)}), f32[1024,8,30]{0,2,1:T(8,128)S(1)}, u32[]{:S(2)}, u32[]{:S(2)}) async-start(f32[1024,8,30]{0,2,1:T(8,128)} %reshape.78), calls=%async_computation.5 | async-start | bytes 2097152 | tf_op jit(solution)/shard_map/all_to_all | solution.py:76
Sparse Core Ops, SparseCore 0:
  428.3 23.8 all-gather.1
  620.4 42.0 reduce-scatter.1
where the time goes:
time: 728 us; the launch traced here: 727 us
  waiting for transfers between devices  581 us (80%)
  other arithmetic  45 us (6%)
  local copies, waits for them, and re-layouts  39.2 us (5%)
  starting transfers between devices  29 us (4%)
  matrix products  19.1 us (3%)
  between operations  14.1 us (2%)
    all_to_all x1, waiting for transfers between devices, per_device(): lax.all_to_all(gate_pieces, 'fs', split_axis=0, concat_axis=1, tiled=True)  175 us
    all_to_all x1, waiting for transfers between devices, per_device(): lax.all_to_all(up_pieces, 'fs', split_axis=0, concat_axis=1, tiled=True)  164 us
    all_to_all x1, waiting for transfers between devices, per_device(): lax.all_to_all(down_pieces, 'fs', split_axis=0, concat_axis=1, tiled=True)  148 us
    reduce_scatter x1, waiting for transfers between devices, per_device(): lax.psum_scatter(lax.dot_general(down_matrix, slot_rows, (((1,), (1,)), (...  42.2 us
    all_to_all x1, waiting for transfers between devices, per_device(): lax.all_to_all(summed.reshape(summed.shape[0], fs_count, CAP), 'fs', spli...  25.5 us
    all_gather x1, waiting for transfers between devices, per_device(): segment = lax.all_gather(arrived, 'tp', axis=2, tiled=True)  25.3 us
    unnamed x9, local copies, waits for them, and re-layouts  24.1 us
    another operation x2, other arithmetic  15.7 us
  transfers between devices with their start and end apart: 7, of which 6 were waited for; matrix products, arithmetic and copies ran while one was open for 8% of the time, Pallas kernels for 0%

commit v1 on v0

v1 whole, which is shorter than its diff:
```python
import functools

import jax
import jax.numpy as jnp
from jax import lax
from jax.experimental import pallas as pl
from jax.experimental.pallas import tpu as pltpu
from jax.sharding import PartitionSpec as P

VMEM_LIMIT = 40 * 1024 * 1024


def fold_kernel(w_ref, gain_ref, out_ref):
    out_ref[...] = (w_ref[...] * gain_ref[...][None]).astype(jnp.bfloat16)


def cast_kernel(w_ref, out_ref):
    out_ref[...] = w_ref[...].astype(jnp.bfloat16)


def arrange(weight, gain, spread, piece, pieces):
    experts, width, columns = weight.shape
    block, rows = columns // spread, width // pieces
    in_specs = [pl.BlockSpec((1, rows, block), lambda e, s: (e, piece, s))]
    operands = [weight]
    if gain is not None:
        in_specs.append(pl.BlockSpec((rows, 1), lambda e, s: (piece, 0)))
        operands.append(gain)
    return pl.pallas_call(
        cast_kernel if gain is None else fold_kernel,
        grid=(experts, spread),
        in_specs=in_specs,
        out_specs=pl.BlockSpec((1, rows, block), lambda e, s: (e * spread + s, 0, 0)),
        out_shape=jax.ShapeDtypeStruct((experts * spread, rows, block), jnp.bfloat16),
        compiler_params=pltpu.CompilerParams(vmem_limit_bytes=VMEM_LIMIT),
        cost_estimate=pl.CostEstimate(
            flops=experts * rows * columns,
            bytes_accessed=experts * rows * columns * 6,
            transcendentals=0,
        ),
    )(*operands)


def gate_kernel(x_ref, w_ref, act_ref, copy_ref):
    copy_ref[...] = w_ref[...]
    part = jnp.dot(x_ref[...], w_ref[0], preferred_element_type=jnp.float32)

    @pl.when(pl.program_id(0) == 0)
    def _():
        act_ref[...] = part

    @pl.when(pl.program_id(0) > 0)
    def _():
        act_ref[...] += part


def up_kernel(x_ref, w_ref, gate_ref, hidden_ref, copy_ref, acc_ref):
    copy_ref[...] = w_ref[...]
    part = jnp.dot(x_ref[...], w_ref[0], preferred_element_type=jnp.float32)

    @pl.when(pl.program_id(0) == 0)
    def _():
        acc_ref[...] = part

    @pl.when(pl.program_id(0) > 0)
    def _():
        acc_ref[...] += part

    @pl.when(pl.program_id(0) == pl.num_programs(0) - 1)
    def _():
        gate = gate_ref[...]
        hidden_ref[...] = (gate / (1.0 + jnp.exp(-gate)) * acc_ref[...]).astype(jnp.bfloat16)


def project(rows, local, gate_act=None):
    count, width, block = local.shape
    tokens = rows.shape[0]
    in_specs = [
        pl.BlockSpec((tokens, width), lambda g: (0, g)),
        pl.BlockSpec((1, width, block), lambda g: (g, 0, 0)),
    ]
    operands = [rows, local]
    scratch = []
    kernel, act_type = gate_kernel, jnp.float32
    if gate_act is not None:
        in_specs.append(pl.BlockSpec((tokens, block), lambda g: (0, 0)))
        operands.append(gate_act)
        scratch = [pltpu.VMEM((tokens, block), jnp.float32)]
        kernel, act_type = up_kernel, jnp.bfloat16
    return pl.pallas_call(
        kernel,
        grid=(count,),
        in_specs=in_specs,
        out_specs=[
            pl.BlockSpec((tokens, block), lambda g: (0, 0)),
            pl.BlockSpec((1, width, block), lambda g: (0, g, 0)),
        ],
        out_shape=[
            jax.ShapeDtypeStruct((tokens, block), act_type),
            jax.ShapeDtypeStruct((1, count * width, block), jnp.bfloat16),
        ],
        scratch_shapes=scratch,
        compiler_params=pltpu.CompilerParams(vmem_limit_bytes=VMEM_LIMIT),
        cost_estimate=pl.CostEstimate(
            flops=2 * tokens * count * width * block,
            bytes_accessed=count * width * block * 4,
            transcendentals=0,
        ),
    )(*operands)


def down_kernel(hidden_ref, weight_ref, w_ref, *rest):
    part_ref, copy_ref = rest[-2:]
    copy_ref[...] = w_ref[...]
    part = lax.dot_general(
        hidden_ref[...], w_ref[0], (((1,), (1,)), ((), ())), preferred_element_type=jnp.float32
    )
    part = part * weight_ref[...]
    part_ref[...] = part.reshape(part_ref.shape).astype(part_ref.dtype)


def project_back(hidden, weight, local, so_far, piece, pieces, fs_count, tp_count, part_type):
    count, width, block = local.shape
    tokens = hidden.shape[0]
    per_tp = count // tp_count
    in_specs = [
        pl.BlockSpec((tokens, block), lambda g: (0, 0)),
        pl.BlockSpec((tokens, 1), lambda g: (0, 0)),
        pl.BlockSpec((1, width, block), lambda g: (g, 0, 0)),
    ]
    operands = [hidden, weight, local]
    aliases = {}
    if so_far is not None:
        in_specs.append(pl.BlockSpec(memory_space=pl.ANY))
        operands.append(so_far)
        aliases = {3: 1}
    return pl.pallas_call(
        down_kernel,
        grid=(count,),
        in_specs=in_specs,
        out_specs=[
            pl.BlockSpec(
                (fs_count, 1, tokens // fs_count, width),
                lambda g: (0, g // per_tp, 0, g % per_tp),
            ),
            pl.BlockSpec((1, width, block), lambda g: (0, g * pieces + piece, 0)),
        ],
        out_shape=[
            jax.ShapeDtypeStruct(
                (fs_count, tp_count, tokens // fs_count, per_tp * width), part_type
            ),
            jax.ShapeDtypeStruct((1, count * width * pieces, block), jnp.bfloat16),
        ],
        input_output_aliases=aliases,
        compiler_params=pltpu.CompilerParams(vmem_limit_bytes=VMEM_LIMIT),
        cost_estimate=pl.CostEstimate(
            flops=2 * tokens * count * width * block,
            bytes_accessed=count * width * block * 4 + tokens * count * width * 4,
            transcendentals=0,
        ),
    )(*operands)


def swap(pieces):
    return lax.all_to_all(pieces, "fs", split_axis=0, concat_axis=0, tiled=True)


def per_device(tokens, routes, route_logits, norm_gain, gate_weight, up_weight, down_weight):
    experts, width, _ = gate_weight.shape
    fs_count, tp_count = lax.axis_size("fs"), lax.axis_size("tp")
    spread = fs_count // experts
    own, model = tokens.shape
    part_width = model // tp_count
    pieces = 2 if width % 256 == 0 else 1
    gain = norm_gain[:, None]

    gate_local = swap(arrange(gate_weight, gain, spread, 0, 1))
    up_pieces = arrange(up_weight, gain, spread, 0, 1)
    down_pieces = [arrange(down_weight, None, spread, p, pieces) for p in range(pieces)]

    tok_float = tokens.astype(jnp.float32)
    scale = lax.rsqrt(jnp.mean(tok_float * tok_float, axis=1, keepdims=True) + 1e-05)
    start = lax.axis_index("tp") * part_width
    own_cols = lax.dynamic_slice_in_dim(tokens, start, part_width, 1).astype(jnp.float32)
    normed = (own_cols * scale).astype(jnp.bfloat16)
    gathered = lax.all_gather(normed, ("fs", "tp"), axis=0, tiled=False)
    rows = (
        gathered.reshape(fs_count, tp_count, own, part_width)
        .transpose(0, 2, 1, 3)
        .reshape(fs_count * own, model)
    )
    shares = jax.nn.sigmoid(route_logits - route_logits[:, ::-1])
    expert_ids = lax.broadcasted_iota(jnp.int32, (1, 1, experts), 2)
    weights = jnp.sum(jnp.where(routes[:, :, None] == expert_ids, shares[:, :, None], 0.0), axis=1)
    all_weights = lax.all_gather(weights, "fs", axis=0, tiled=True)
    mine = lax.axis_index("fs") // spread
    weight = lax.dynamic_slice_in_dim(all_weights, mine, 1, 1)

    up_local = swap(up_pieces)
    gate_act, gate_out = project(rows, gate_local)
    hidden, up_out = project(rows, up_local, gate_act)
    down_out, sums = None, []
    for p in range(pieces):
        part, down_out = project_back(
            hidden, weight, swap(down_pieces[p]), down_out, p, pieces, fs_count, tp_count, jnp.float32
        )
        part = part.reshape((fs_count * tp_count,) + part.shape[2:])
        summed = lax.psum_scatter(part, ("fs", "tp"), scatter_dimension=0, tiled=True)
        sums.append(summed.reshape(own, part_width // width, 1, width // pieces))
    mixed = jnp.concatenate(sums, axis=2).reshape(own, part_width).astype(jnp.bfloat16)
    return (mixed, gate_out, up_out, down_out)


def solution(mesh):
    in_specs = (
        P("fs", None),
        P("fs", None),
        P("fs", None),
        P("fs"),
        P(None, "fs", "tp"),
        P(None, "fs", "tp"),
        P(None, "fs", "tp"),
    )
    out_specs = (P("fs", "tp"), P("tp", None, "fs"), P("tp", None, "fs"), P("tp", None, "fs"))
    return jax.shard_map(
        per_device, mesh=mesh, in_specs=in_specs, out_specs=out_specs, check_vma=False
    )
```

time: 728 us -> 937 us (1.29)
  blocking collectives: 0 us -> 118 us
  waiting for transfers between devices: 581 us -> 695 us
  Pallas kernels: 0 us -> 66.2 us
  other arithmetic: 45 us -> 2.91 us
  local copies, waits for them, and re-layouts: 39.2 us -> 16.8 us
  matrix products: 19.1 us -> 0 us
    reduce_scatter x1 -> x2, waiting for transfers between devices: 42.2 us -> 265 us  [per_device(): lax.psum_scatter(part, ('fs', 'tp'), scatter_dimension=0, tiled=True)]
    all_gather x0 -> x1, blocking collectives: none -> 118 us  [per_device(): all_weights = lax.all_gather(weights, 'fs', axis=0, tiled=True)]
    all_to_all x5 -> x4, waiting for transfers between devices: 512 us -> 431 us  [swap(): return lax.all_to_all(pieces, 'fs', split_axis=0, concat_axis=0, tiled=True)]
    pallas_call x0 -> x8, Pallas kernels: none -> 66.2 us  [the longest x4 27.8 us: arrange(): pl.pallas_call(cast_kernel if gain is None else fold_kernel, grid=(expert...]
    all_gather x1, waiting for transfers between devices: 25.3 us -> 0.02 us  [per_device(): gathered = lax.all_gather(normed, ('fs', 'tp'), axis=0, tiled=False)]
    dot_general x4 -> x0, matrix products: 19.1 us -> none  [the longest x1 12.2 us: per_device(): lax.dot_general(down_matrix, slot_rows, (((1,), (1,)), ((), ())), preferr...]
    convert_element_type x3 -> x1, other arithmetic: 19.5 us -> 0.72 us  [per_device(): normed = (own_cols * scale).astype(jnp.bfloat16)]
    another operation x3 -> x2, other arithmetic: 15.7 us -> 1.79 us
  transfers between devices with their start and end apart: 7 -> 7, of which waited for: 6 -> 5; matrix products, arithmetic and copies ran while one was open for 8% -> 1% of each run, Pallas kernels for 0% -> 6%
where the time goes in v1:
time: 937 us; the launch traced here: 935 us
  waiting for transfers between devices  695 us (74%)
  blocking collectives  118 us (13%)
  Pallas kernels  66.2 us (7%)
  starting transfers between devices  22.1 us (2%)
  local copies, waits for them, and re-layouts  16.8 us (2%)
  between operations  13.9 us (1%)
    all_to_all x4, waiting for transfers between devices, swap(): return lax.all_to_all(pieces, 'fs', split_axis=0, concat_axis=0, tiled=True)  431 us
    reduce_scatter x2, waiting for transfers between devices, per_device(): lax.psum_scatter(part, ('fs', 'tp'), scatter_dimension=0, tiled=True)  265 us
    all_gather x1, blocking collectives, per_device(): all_weights = lax.all_gather(weights, 'fs', axis=0, tiled=True)  118 us
    pallas_call x4, Pallas kernels, arrange(): pl.pallas_call(cast_kernel if gain is None else fold_kernel, grid=(expert...  27.8 us
    all_to_all x4, starting transfers between devices, swap(): return lax.all_to_all(pieces, 'fs', split_axis=0, concat_axis=0, tiled=True)  21.9 us
    pallas_call x2, Pallas kernels, project(): pl.pallas_call(kernel, grid=(count,), in_specs=in_specs, out_specs=[pl.Bl...  21.8 us
  transfers between devices with their start and end apart: 7, of which 5 were waited for; matrix products, arithmetic and copies ran while one was open for 1% of the time, Pallas kernels for 6%

profile of v1, /device:TPU:0, one launch (start us, length us, event | category | flops | bytes accessed | tf_op | source)
XLA Modules:
  0.0 935.0 jit_solution(13170088904063274367)
XLA Ops:
  7.2 5.7 shard_map.106
  12.9 0.0 copy-start.3
  12.9 2.0 copy-done.3
  14.9 7.4 all-to-all-start.2
  22.3 0.0 copy-done.6
  22.3 0.1 copy.33.gain_ref
  22.4 8.2 shard_map.103
  30.6 0.0 copy-start.1
  30.7 3.4 copy-done.1
  34.0 81.5 %all-to-all-done.2.w_ref = bf16[8,256,1024]{2,1,0:T(8,128)(2,1)} async-done(((bf16[8,256,1024]{2,1,0:T(8,128)(2,1)}), bf16[8,256,1024]{2,1,0:T(8,128)(2,1)}, u32[]{:S(2)}, u32[]{:S(2)}) %all-to-all-start.2) | async-done | bytes 4194336 | tf_op jit(solution)/shard_map/all_to_all | solution.py:165
  115.6 5.0 all-to-all-start.1
  120.6 8.2 shard_map.102
  128.8 0.0 copy-start
  128.8 3.4 copy-done
  132.2 170.6 %all-to-all-done.1.w_ref = bf16[8,512,1024]{2,1,0:T(8,128)(2,1)} async-done(((bf16[8,512,1024]{2,1,0:T(8,128)(2,1)}), bf16[8,512,1024]{2,1,0:T(8,128)(2,1)}, u32[]{:S(2)}, u32[]{:S(2)}) %all-to-all-start.1) | async-done | bytes 8388640 | tf_op jit(solution)/shard_map/all_to_all | solution.py:165
  302.9 5.0 all-to-all-start
  307.8 0.0 all-gather.4.cloned.1.call-start
  307.9 0.0 copy-done.4
  307.9 0.2 multiply_reduce_fusion
  308.1 0.7 multiply_convert_fusion
  308.8 0.0 all-gather.4.cloned.1.call-update
  308.8 5.7 shard_map.108
  314.5 2.0 copy-done.2
  316.5 178.7 %all-to-all-done.w_ref = bf16[8,512,1024]{2,1,0:T(8,128)(2,1)} async-done(((bf16[8,512,1024]{2,1,0:T(8,128)(2,1)}), bf16[8,512,1024]{2,1,0:T(8,128)(2,1)}, u32[]{:S(2)}, u32[]{:S(2)}) %all-to-all-start) | async-done | bytes 8388640 | tf_op jit(solution)/shard_map/all_to_all | solution.py:165
  495.2 4.5 all-to-all-start.3
  499.7 0.0 reduce-scatter.3.cloned.1.call-start
  499.8 0.0 copy-done.5
  499.9 0.0 copy-done.7
  499.9 117.5 %all-gather.1 = f32[8,40,4]{1,2,0:T(4,128)S(1)} all-gather(f32[1,40,4]{1,2,0:T(4,128)S(1)} %bitcast.15), channel_id=1, replica_groups=mesh['fs'=8,'tp'=4] {'fs'}, dimensions={0}, use_global_device_ids=true | all-gather | bytes 5760 | tf_op jit(solution)/shard_map/all_gather | solution.py:195
  617.4 0.1 copy.35
  617.6 0.1 constant_dynamic-slice_fusion.weight_ref
  617.7 0.0 all-gather.4.cloned.1.call-done
  617.7 3.8 copy.32
  621.5 1.1 copy.38
  622.6 10.7 %shard_map.104 = (f32[320,1024]{1,0:T(8,128)S(1)}, bf16[1,4096,1024]{2,1,0:T(8,128)(2,1)}) custom-call(bf16[320,4096]{1,0:T(8,128)(2,1)S(1)} %bitcast.10, bf16[8,512,1024]{2,1,0:T(8,128)(2,1)} %all-to-all-done.1.w_ref), custom_call_target="tpu_custom_call" | custom-call | flops 2684354560 | bytes 16777216 | tf_op jit(solution)/shard_map/pallas_call | solution.py:90
  633.3 11.1 %shard_map.105 = (bf16[320,1024]{1,0:T(8,128)(2,1)S(1)}, bf16[1,4096,1024]{2,1,0:T(8,128)(2,1)}) custom-call(bf16[320,4096]{1,0:T(8,128)(2,1)S(1)} %bitcast.11, bf16[8,512,1024]{2,1,0:T(8,128)(2,1)} %all-to-all-done.w_ref, f32[320,1024]{1,0:T(8,128)S(1)} %get-tuple-element.12.gate_ref), custom_call_target="tpu_custom_call" | custom-call | flops 2684354560 | bytes 16777216 | tf_op jit(solution)/shard_map/pallas_call | solution.py:90
  644.4 8.3 shard_map.107
  652.7 0.0 reduce-scatter.3.cloned.1.call-update
  652.7 0.0 reduce-scatter.5.cloned.1.call-start
  652.8 0.0 all-to-all-done.3.w_ref
  652.8 8.4 shard_map.109
  661.2 0.0 reduce-scatter.5.cloned.1.call-update
  661.2 128.2 %reduce-scatter.3.cloned.1.call-done = f32[1,40,512]{2,1,0:T(8,128)} async-done(((f32[32,40,512]{2,1,0:T(8,128)}), f32[1,40,512]{2,1,0:T(8,128)}) %reduce-scatter.3.cloned.1.call-update) | async-done | bytes 81936 | tf_op jit(solution)/shard_map/reduce_scatter | solution.py:208
  789.3 0.9 convert.8
  790.3 136.4 %reduce-scatter.5.cloned.1.call-done = f32[1,40,512]{2,1,0:T(8,128)} async-done(((f32[32,40,512]{2,1,0:T(8,128)}), f32[1,40,512]{2,1,0:T(8,128)}) %reduce-scatter.5.cloned.1.call-update) | async-done | bytes 81936 | tf_op jit(solution)/shard_map/reduce_scatter | solution.py:208
  926.6 0.9 convert.9
  927.6 0.2 pad_maximum_fusion
  927.8 0.7 convert_element_type.16
  (11 shorter events, 0.1 us)
Async XLA Ops:
  12.9 2.0 copy-start.3
  14.9 7.4 copy-start.6
  14.9 100.7 %all-to-all-start.2 = ((bf16[8,256,1024]{2,1,0:T(8,128)(2,1)}), bf16[8,256,1024]{2,1,0:T(8,128)(2,1)}, u32[]{:S(2)}, u32[]{:S(2)}) async-start(bf16[8,256,1024]{2,1,0:T(8,128)(2,1)} %copy-done.3), calls=%async_computation.2 | async-start | bytes 8388608 | tf_op jit(solution)/shard_map/all_to_all | solution.py:165
  30.6 3.4 copy-start.1
  115.6 187.3 %all-to-all-start.1 = ((bf16[8,512,1024]{2,1,0:T(8,128)(2,1)}), bf16[8,512,1024]{2,1,0:T(8,128)(2,1)}, u32[]{:S(2)}, u32[]{:S(2)}) async-start(bf16[8,512,1024]{2,1,0:T(8,128)(2,1)} %copy-done.1), calls=%async_computation.1 | async-start | bytes 16777216 | tf_op jit(solution)/shard_map/all_to_all | solution.py:165
  128.8 3.4 copy-start
  132.2 175.7 %copy-start.4 = (bf16[40,4096]{1,0:T(8,128)(2,1)S(1)}, bf16[40,4096]{1,0:T(8,128)(2,1)}, u32[]{:S(2)}) copy-start(bf16[40,4096]{1,0:T(8,128)(2,1)} %param.7) | copy-start | bytes 983044
  302.9 192.3 %all-to-all-start = ((bf16[8,512,1024]{2,1,0:T(8,128)(2,1)}), bf16[8,512,1024]{2,1,0:T(8,128)(2,1)}, u32[]{:S(2)}, u32[]{:S(2)}) async-start(bf16[8,512,1024]{2,1,0:T(8,128)(2,1)} %copy-done), calls=%async_computation | async-start | bytes 16777216 | tf_op jit(solution)/shard_map/all_to_all | solution.py:165
  307.8 309.9 %all-gather.4.cloned.1.call-start = ((), (), s32[]{:S(2)}) async-start(), calls=%async_computation.8 | async-start | bytes 2703360 | tf_op jit(solution)/shard_map/all_gather | solution.py:186
  314.5 2.0 copy-start.2
  316.5 183.3 %copy-start.5 = (f32[40,2]{0,1:T(2,128)S(1)}, f32[40,2]{0,1:T(2,128)}, u32[]{:S(2)}) copy-start(f32[40,2]{0,1:T(2,128)} %param.9) | copy-start | bytes 964
  316.5 183.4 %copy-start.7 = (s32[40,2]{0,1:T(2,128)S(1)}, s32[40,2]{0,1:T(2,128)}, u32[]{:S(2)}) copy-start(s32[40,2]{0,1:T(2,128)} %param.8) | copy-start | bytes 964
  495.2 157.6 %all-to-all-start.3 = ((bf16[8,256,1024]{2,1,0:T(8,128)(2,1)}), bf16[8,256,1024]{2,1,0:T(8,128)(2,1)}, u32[]{:S(2)}, u32[]{:S(2)}) async-start(bf16[8,256,1024]{2,1,0:T(8,128)(2,1)} %copy-done.2), calls=%async_computation.4 | async-start | bytes 8388608 | tf_op jit(solution)/shard_map/all_to_all | solution.py:165
  499.7 289.6 %reduce-scatter.3.cloned.1.call-start = ((), (), s32[]{:S(2)}) async-start(), calls=%async_computation.6 | async-start | bytes 2703360 | tf_op jit(solution)/shard_map/reduce_scatter | solution.py:208
  652.7 273.9 %reduce-scatter.5.cloned.1.call-start = ((), (), s32[]{:S(2)}) async-start(), calls=%async_computation.7 | async-start | bytes 2703360 | tf_op jit(solution)/shard_map/reduce_scatter | solution.py:208
Sparse Core Ops, SparseCore 0:
  312.1 225.1 all-gather.3
  652.8 136.4 reduce-scatter.2
  791.6 134.9 reduce-scatter.4

commit v2 on v1

v2 whole, which is shorter than its diff:
```python
import functools

import jax
import jax.numpy as jnp
from jax import lax
from jax.experimental import pallas as pl
from jax.experimental.pallas import tpu as pltpu
from jax.sharding import PartitionSpec as P

VMEM_LIMIT = 40 * 1024 * 1024


MESH = pl.DeviceIdType.MESH


def exchange_kernel(
    fs_count, tp_count, experts, pieces,
    tok_ref, routes_ref, logits_ref, gain_ref, gate_hbm, up_hbm, down_hbm,
    rows_out, weights_out, gate_out, up_out, down_out, rest_out,
    xcol, wown, stage, gate_send, up_send, down_send, rest_send,
    load_sem, send_sem, recv_sem, keep_sem, x_send, x_recv, w_send, w_recv, t_send, t_recv,
    own_sem, rest_sem,
):
    me, my_tp = lax.axis_index("fs"), lax.axis_index("tp")
    spread = fs_count // experts
    own = tok_ref.shape[0]
    width, block = stage.shape[1], stage.shape[2]
    part = xcol.shape[2]
    rows = width // pieces
    barrier = pltpu.get_barrier_semaphore()
    for s in range(1, fs_count):
        pl.semaphore_signal(
            barrier, inc=1, device_id={"fs": lax.rem(me + s, fs_count)}, device_id_type=MESH
        )
    for s in range(1, tp_count):
        pl.semaphore_signal(
            barrier, inc=1, device_id={"tp": lax.rem(my_tp + s, tp_count)}, device_id_type=MESH
        )

    def target(step):
        return lax.rem(me + fs_count // 2 + step, fs_count)

    def load(hbm, step, slot):
        dst = target(step)
        column = pl.multiple_of(lax.rem(dst, spread) * block, block)
        return pltpu.make_async_copy(
            hbm.at[dst // spread, :, pl.ds(column, block)], stage.at[slot], load_sem.at[slot]
        )

    load(gate_hbm, 0, 0).start()

    tok = tok_ref[...].astype(jnp.float32)
    scale = lax.rsqrt(jnp.mean(tok * tok, axis=1, keepdims=True) + 1e-05)
    cols = tok_ref[:, pl.ds(pl.multiple_of(my_tp * part, part), part)].astype(jnp.float32)
    xcol[me] = (cols * scale).astype(jnp.bfloat16)
    first, second = logits_ref[:, 0:1], logits_ref[:, 1:2]
    lanes = lax.broadcasted_iota(jnp.int32, (own, 128), 1)
    wown[...] = jnp.where(
        routes_ref[:, 0:1] == lanes, 1.0 / (1.0 + jnp.exp(second - first)), 0.0
    ) + jnp.where(routes_ref[:, 1:2] == lanes, 1.0 / (1.0 + jnp.exp(first - second)), 0.0)
    pl.semaphore_wait(barrier, fs_count + tp_count - 2)

    def x_copy(dst, sem):
        return pltpu.make_async_remote_copy(
            src_ref=xcol.at[me], dst_ref=xcol.at[me], send_sem=x_send.at[dst],
            recv_sem=x_recv.at[sem], device_id={"fs": dst}, device_id_type=MESH,
        )

    def w_copy(dst, sem):
        return pltpu.make_async_remote_copy(
            src_ref=wown, dst_ref=weights_out.at[me], send_sem=w_send.at[dst],
            recv_sem=w_recv.at[sem], device_id={"fs": dst}, device_id_type=MESH,
        )

    w_keep = pltpu.make_async_copy(wown, weights_out.at[me], own_sem.at[0])
    w_keep.start()
    for s in range(1, fs_count):
        dst = lax.rem(me + s, fs_count)
        x_copy(dst, me).start()
        w_copy(dst, me).start()

    weights_in = (
        (gate_hbm, gate_send, gate_out, True),
        (up_hbm, up_send, up_out, True),
        (down_hbm, down_send, down_out, False),
    )

    def w_send_copy(m, dst):
        _, held, out, _ = weights_in[m]
        return pltpu.make_async_remote_copy(
            src_ref=held.at[dst], dst_ref=out.at[me], send_sem=send_sem.at[m, dst],
            recv_sem=recv_sem.at[m, me], device_id={"fs": dst}, device_id_type=MESH,
        )

    def keep_copy(m):
        _, held, out, _ = weights_in[m]
        return pltpu.make_async_copy(held.at[me], out.at[me], keep_sem.at[m])

    t_copies = []
    for m in range(3):
        hbm, held, out, folded = weights_in[m]

        def body(step, carry, m=m, hbm=hbm, held=held, folded=folded):
            slot = lax.rem(m * fs_count + step, 2)
            dst = target(step)

            @pl.when(step + 1 < fs_count)
            def _():
                load(hbm, step + 1, 1 - slot).start()

            if m < 2:

                @pl.when(step + 1 == fs_count)
                def _():
                    load(weights_in[m + 1][0], 0, 1 - slot).start()

            load(hbm, step, slot).wait()
            if folded:
                held[dst] = (stage[slot] * gain_ref[...]).astype(jnp.bfloat16)
            else:
                held[dst] = stage[slot, :rows].astype(jnp.bfloat16)
                if pieces > 1:
                    rest_send[dst] = stage[slot, rows:].astype(jnp.bfloat16)

            @pl.when(dst == me)
            def _():
                keep_copy(m).start()

            @pl.when(dst != me)
            def _():
                w_send_copy(m, dst).start()

            return carry

        lax.fori_loop(0, fs_count, body, 0)
        if m == 0:
            for s in range(1, fs_count):
                src = lax.rem(me + s, fs_count)
                pltpu.make_async_copy(xcol.at[src], xcol.at[src], x_recv.at[src]).wait()
            for s in range(1, tp_count):
                copy = pltpu.make_async_remote_copy(
                    src_ref=xcol, dst_ref=rows_out.at[my_tp], send_sem=t_send.at[s],
                    recv_sem=t_recv.at[s], device_id={"tp": lax.rem(my_tp + s, tp_count)},
                    device_id_type=MESH,
                )
                copy.start()
                t_copies.append(copy)
            x_keep = pltpu.make_async_copy(xcol, rows_out.at[my_tp], own_sem.at[1])
            x_keep.start()
    if pieces > 1:
        rest_copy = pltpu.make_async_copy(rest_send, rest_out, rest_sem)
        rest_copy.start()
        rest_copy.wait()
    w_keep.wait()
    x_keep.wait()
    for s in range(1, tp_count):
        src = lax.rem(my_tp + tp_count - s, tp_count)
        t_copies[s - 1].wait_send()
        pltpu.make_async_copy(xcol, rows_out.at[src], t_recv.at[s]).wait()
    for s in range(1, fs_count):
        other = lax.rem(me + s, fs_count)
        x_copy(other, me).wait_send()
        w_copy(other, me).wait_send()
        pltpu.make_async_copy(wown, weights_out.at[other], w_recv.at[other]).wait()
    for m in range(3):
        _, held, out, _ = weights_in[m]
        keep_copy(m).wait()

        def finish(s, carry, m=m, held=held, out=out):
            other = lax.rem(me + s, fs_count)
            w_send_copy(m, other).wait_send()
            pltpu.make_async_copy(held.at[other], out.at[other], recv_sem.at[m, other]).wait()
            return carry

        lax.fori_loop(1, fs_count, finish, 0)


def exchange(tokens, routes, logits, gain, gate, up, down, fs_count, tp_count, pieces):
    experts, width, columns = gate.shape
    block = columns // (fs_count // experts)
    rows = width // pieces
    own, model = tokens.shape
    part = model // tp_count
    bf16, dma = jnp.bfloat16, pltpu.SemaphoreType.DMA
    vmem = pl.BlockSpec(memory_space=pltpu.VMEM)
    anywhere = pl.BlockSpec(memory_space=pl.ANY)
    return pl.pallas_call(
        functools.partial(exchange_kernel, fs_count, tp_count, experts, pieces),
        in_specs=[vmem] * 4 + [anywhere] * 3,
        out_specs=[anywhere] * 6,
        out_shape=[
            jax.ShapeDtypeStruct((tp_count, fs_count, own, part), bf16),
            jax.ShapeDtypeStruct((fs_count, own, 128), jnp.float32),
            jax.ShapeDtypeStruct((fs_count, width, block), bf16),
            jax.ShapeDtypeStruct((fs_count, width, block), bf16),
            jax.ShapeDtypeStruct((fs_count, rows, block), bf16),
            jax.ShapeDtypeStruct((fs_count, rows, block), bf16),
        ],
        scratch_shapes=[
            pltpu.VMEM((fs_count, own, part), bf16),
            pltpu.VMEM((own, 128), jnp.float32),
            pltpu.VMEM((2, width, block), jnp.float32),
            pltpu.VMEM((fs_count, width, block), bf16),
            pltpu.VMEM((fs_count, width, block), bf16),
            pltpu.VMEM((fs_count, rows, block), bf16),
            pltpu.VMEM((fs_count, rows, block), bf16),
            dma((2,)), dma((3, fs_count)), dma((3, fs_count)), dma((3,)),
            dma((fs_count,)), dma((fs_count,)), dma((fs_count,)), dma((fs_count,)),
            dma((tp_count,)), dma((tp_count,)), dma((2,)), dma,
        ],
        compiler_params=pltpu.CompilerParams(
            collective_id=0, has_side_effects=True, vmem_limit_bytes=56 * 1024 * 1024
        ),
    )(tokens, routes, logits, gain, gate, up, down)


def reduce_kernel(
    fs_count, tp_count, experts, part_ref, out_ref, first, total, second,
    send1, recv1, send2, recv2, keep_sem,
):
    me, my_tp = lax.axis_index("fs"), lax.axis_index("tp")
    spread = fs_count // experts
    mine, half = me // spread, lax.rem(me, spread)
    group = spread * tp_count
    index = half * tp_count + my_tp
    barrier = pltpu.get_barrier_semaphore()

    def mate(s):
        other = lax.rem(index + s, group)
        return other, other // tp_count, lax.rem(other, tp_count)

    def partner(s):
        return lax.rem(mine + s, experts)

    for s in range(1, group):
        _, h, t = mate(s)
        pl.semaphore_signal(
            barrier, inc=1, device_id={"fs": mine * spread + h, "tp": t}, device_id_type=MESH
        )
    for s in range(1, experts):
        pl.semaphore_signal(
            barrier, inc=1, device_id={"fs": partner(s) * spread + half}, device_id_type=MESH
        )
    pl.semaphore_wait(barrier, group + experts - 2)

    def copy1(s):
        _, h, t = mate(s)
        return pltpu.make_async_remote_copy(
            src_ref=part_ref.at[h, t], dst_ref=first.at[s], send_sem=send1.at[s],
            recv_sem=recv1.at[s], device_id={"fs": mine * spread + h, "tp": t},
            device_id_type=MESH,
        )

    for s in range(1, group):
        copy1(s).start()
    keep = pltpu.make_async_copy(part_ref.at[half, my_tp], first.at[0], keep_sem)
    keep.start()
    keep.wait()
    acc = first[0].astype(jnp.float32)
    for s in range(1, group):
        copy1(s).wait_recv()
        acc = acc + first[s].astype(jnp.float32)
    total[...] = acc.astype(jnp.bfloat16)

    def copy2(s):
        return pltpu.make_async_remote_copy(
            src_ref=total.at[partner(s)], dst_ref=second.at[s], send_sem=send2.at[s],
            recv_sem=recv2.at[s], device_id={"fs": partner(s) * spread + half},
            device_id_type=MESH,
        )

    for s in range(1, experts):
        copy2(s).start()
    result = total[mine].astype(jnp.float32)
    for s in range(1, experts):
        copy2(s).wait_recv()
        result = result + second[s].astype(jnp.float32)
    out_ref[...] = result.astype(jnp.bfloat16)
    for s in range(1, group):
        copy1(s).wait_send()
    for s in range(1, experts):
        copy2(s).wait_send()


def reduce(part, fs_count, tp_count):
    spread, _, experts, own, columns = part.shape
    group = spread * tp_count
    bf16, dma = jnp.bfloat16, pltpu.SemaphoreType.DMA
    return pl.pallas_call(
        functools.partial(reduce_kernel, fs_count, tp_count, experts),
        in_specs=[pl.BlockSpec(memory_space=pltpu.VMEM)],
        out_specs=pl.BlockSpec(memory_space=pltpu.VMEM),
        out_shape=jax.ShapeDtypeStruct((own, columns), bf16),
        scratch_shapes=[
            pltpu.VMEM((group, experts, own, columns), bf16),
            pltpu.VMEM((experts, own, columns), bf16),
            pltpu.VMEM((experts, own, columns), bf16),
            dma((group,)), dma((group,)), dma((experts,)), dma((experts,)), dma,
        ],
        compiler_params=pltpu.CompilerParams(
            collective_id=1, has_side_effects=True, vmem_limit_bytes=48 * 1024 * 1024
        ),
    )(part)


def gate_kernel(x_ref, w_ref, act_ref, copy_ref):
    copy_ref[...] = w_ref[...]
    part = jnp.dot(x_ref[0], w_ref[0], preferred_element_type=jnp.float32)

    @pl.when(pl.program_id(0) == 0)
    def _():
        act_ref[...] = part

    @pl.when(pl.program_id(0) > 0)
    def _():
        act_ref[...] += part


def up_kernel(x_ref, w_ref, gate_ref, hidden_ref, copy_ref, acc_ref):
    copy_ref[...] = w_ref[...]
    part = jnp.dot(x_ref[0], w_ref[0], preferred_element_type=jnp.float32)

    @pl.when(pl.program_id(0) == 0)
    def _():
        acc_ref[...] = part

    @pl.when(pl.program_id(0) > 0)
    def _():
        acc_ref[...] += part

    @pl.when(pl.program_id(0) == pl.num_programs(0) - 1)
    def _():
        gate = gate_ref[...]
        hidden_ref[...] = (gate / (1.0 + jnp.exp(-gate)) * acc_ref[...]).astype(jnp.bfloat16)


def project(rows, local, gate_act=None):
    count, width, block = local.shape
    tokens = rows.shape[1]
    per_tp = count // rows.shape[0]
    in_specs = [
        pl.BlockSpec((1, tokens, width), lambda g: (g // per_tp, 0, g % per_tp)),
        pl.BlockSpec((1, width, block), lambda g: (g, 0, 0)),
    ]
    operands = [rows, local]
    scratch = []
    kernel, act_type = gate_kernel, jnp.float32
    if gate_act is not None:
        in_specs.append(pl.BlockSpec((tokens, block), lambda g: (0, 0)))
        operands.append(gate_act)
        scratch = [pltpu.VMEM((tokens, block), jnp.float32)]
        kernel, act_type = up_kernel, jnp.bfloat16
    return pl.pallas_call(
        kernel,
        grid=(count,),
        in_specs=in_specs,
        out_specs=[
            pl.BlockSpec((tokens, block), lambda g: (0, 0)),
            pl.BlockSpec((1, width, block), lambda g: (0, g, 0)),
        ],
        out_shape=[
            jax.ShapeDtypeStruct((tokens, block), act_type),
            jax.ShapeDtypeStruct((1, count * width, block), jnp.bfloat16),
        ],
        scratch_shapes=scratch,
        compiler_params=pltpu.CompilerParams(vmem_limit_bytes=VMEM_LIMIT),
        cost_estimate=pl.CostEstimate(
            flops=2 * tokens * count * width * block,
            bytes_accessed=count * width * block * 4,
            transcendentals=0,
        ),
    )(*operands)


def down_kernel(hidden_ref, weight_ref, w_ref, *rest):
    part_ref, copy_ref = rest[-2:]
    copy_ref[...] = w_ref[...]
    part = lax.dot_general(
        hidden_ref[...], w_ref[0], (((1,), (1,)), ((), ())), preferred_element_type=jnp.float32
    )
    part = part * weight_ref[...]
    spread, _, experts, own, width = part_ref.shape
    blocks = part.reshape(experts, spread, own, width).astype(part_ref.dtype)
    for h in range(spread):
        part_ref[h, 0] = blocks[:, h]


def project_back(hidden, weight, local, so_far, piece, pieces, experts, spread, tp_count):
    count, width, block = local.shape
    tokens = hidden.shape[0]
    per_tp = count // tp_count
    own = tokens // count
    in_specs = [
        pl.BlockSpec((tokens, block), lambda g: (0, 0)),
        pl.BlockSpec((tokens, 1), lambda g: (0, 0)),
        pl.BlockSpec((1, width, block), lambda g: (g, 0, 0)),
    ]
    operands = [hidden, weight, local]
    aliases = {}
    if so_far is not None:
        in_specs.append(pl.BlockSpec(memory_space=pl.ANY))
        operands.append(so_far)
        aliases = {3: 1}
    return pl.pallas_call(
        down_kernel,
        grid=(count,),
        in_specs=in_specs,
        out_specs=[
            pl.BlockSpec(
                (spread, 1, experts, own, width),
                lambda g: (0, g // per_tp, 0, 0, g % per_tp),
            ),
            pl.BlockSpec((1, width, block), lambda g: (0, g * pieces + piece, 0)),
        ],
        out_shape=[
            jax.ShapeDtypeStruct(
                (spread, tp_count, experts, own, per_tp * width), jnp.bfloat16
            ),
            jax.ShapeDtypeStruct((1, count * width * pieces, block), jnp.bfloat16),
        ],
        input_output_aliases=aliases,
        compiler_params=pltpu.CompilerParams(vmem_limit_bytes=VMEM_LIMIT),
        cost_estimate=pl.CostEstimate(
            flops=2 * tokens * count * width * block,
            bytes_accessed=count * width * block * 4 + tokens * count * width * 4,
            transcendentals=0,
        ),
    )(*operands)


def swap(pieces):
    return lax.all_to_all(pieces, "fs", split_axis=0, concat_axis=0, tiled=True)


def per_device(tokens, routes, route_logits, norm_gain, gate_weight, up_weight, down_weight):
    experts, width, _ = gate_weight.shape
    fs_count, tp_count = lax.axis_size("fs"), lax.axis_size("tp")
    spread = fs_count // experts
    own, model = tokens.shape
    part_width = model // tp_count
    pieces = 2 if width % 256 == 0 else 1
    rows, weights, gate_local, up_local, down_local, rest = exchange(
        tokens, routes, route_logits, norm_gain[:, None],
        gate_weight, up_weight, down_weight, fs_count, tp_count, pieces,
    )
    rows = rows.reshape(tp_count, fs_count * own, part_width)
    mine = lax.axis_index("fs") // spread
    weight = lax.dynamic_slice_in_dim(weights.reshape(fs_count * own, -1), mine, 1, 1)
    locals_ = [down_local]
    if pieces > 1:
        locals_.append(swap(rest))
    gate_act, gate_out = project(rows, gate_local)
    hidden, up_out = project(rows, up_local, gate_act)
    down_out, sums = None, []
    for p in range(pieces):
        part, down_out = project_back(
            hidden, weight, locals_[p], down_out, p, pieces, experts, spread, tp_count
        )
        summed = reduce(part, fs_count, tp_count)
        sums.append(summed.reshape(own, part_width // width, 1, width // pieces))
    mixed = jnp.concatenate(sums, axis=2).reshape(own, part_width)
    return (mixed, gate_out, up_out, down_out)


def solution(mesh):
    in_specs = (
        P("fs", None),
        P("fs", None),
        P("fs", None),
        P("fs"),
        P(None, "fs", "tp"),
        P(None, "fs", "tp"),
        P(None, "fs", "tp"),
    )
    out_specs = (P("fs", "tp"), P("tp", None, "fs"), P("tp", None, "fs"), P("tp", None, "fs"))
    return jax.shard_map(
        per_device, mesh=mesh, in_specs=in_specs, out_specs=out_specs, check_vma=False
    )
```

time: 937 us -> 613 us (0.65)
  waiting for transfers between devices: 695 us -> 0.01 us
  Pallas kernels: 66.2 us -> 593 us
  blocking collectives: 118 us -> 0 us
  starting transfers between devices: 22.1 us -> 4.83 us
  between operations: 13.9 us -> 0.77 us
    pallas_call x4 -> x3, Pallas kernels: 27.8 us -> 565 us  [the longest x1 477 us: exchange(): pl.pallas_call(functools.partial(exchange_kernel, fs_count, tp_count, exp...]
    all_to_all x4 -> x1, waiting for transfers between devices: 431 us -> 0.01 us  [swap(): return lax.all_to_all(pieces, 'fs', split_axis=0, concat_axis=0, tiled=True)]
    reduce_scatter x2 -> x0, waiting for transfers between devices: 265 us -> none  [per_device(): lax.psum_scatter(part, ('fs', 'tp'), scatter_dimension=0, tiled=True)]
    all_gather x1 -> x0, blocking collectives: 118 us -> none  [per_device(): all_weights = lax.all_gather(weights, 'fs', axis=0, tiled=True)]
    all_to_all x4 -> x1, starting transfers between devices: 21.9 us -> 4.83 us  [swap(): return lax.all_to_all(pieces, 'fs', split_axis=0, concat_axis=0, tiled=True)]
  transfers between devices with their start and end apart: 7 -> 1, of which waited for: 5 -> 0; matrix products, arithmetic and copies ran while one was open for 1% -> 0% of each run, Pallas kernels for 6% -> 15%
where the time goes in v2:
time: 613 us; the launch traced here: 611 us
  Pallas kernels  593 us (97%)
  local copies, waits for them, and re-layouts  11.9 us (2%)
    pallas_call x1, Pallas kernels, exchange(): pl.pallas_call(functools.partial(exchange_kernel, fs_count, tp_count, exp...  477 us
    pallas_call x2, Pallas kernels, reduce(): pl.pallas_call(functools.partial(reduce_kernel, fs_count, tp_count, exper...  88.1 us
    pallas_call x2, Pallas kernels, project(): pl.pallas_call(kernel, grid=(count,), in_specs=in_specs, out_specs=[pl.Bl...  15.3 us
    pallas_call x2, Pallas kernels, project_back(): pl.pallas_call(down_kernel, grid=(count,), in_specs=in_specs, out_specs=[...  13.1 us
  transfers between devices with their start and end apart: 1, of which 0 were waited for; matrix products, arithmetic and copies ran while one was open for 0% of the time, Pallas kernels for 15%

profile of v2, /device:TPU:0, one launch (start us, length us, event | category | flops | bytes accessed | tf_op | source)
XLA Modules:
  0.0 611.0 jit_solution(3214226057202407041)
XLA Ops:
  0.6 1.4 copy.15.routes_ref
  2.0 1.4 copy.16.logits_ref
  3.4 1.5 copy.17.gain_ref
  4.9 476.8 %shard_map.102 = (bf16[4,8,40,1024]{3,2,1,0:T(8,128)(2,1)}, f32[8,40,128]{2,1,0:T(8,128)}, bf16[8,512,1024]{2,1,0:T(8,128)(2,1)}, bf16[8,512,1024]{2,1,0:T(8,128...) custom-call(bf16[40,4096]{1,0:T(8,128)(2,1)} %tok_ref.1, s32[40,2]{1,0:T(8,128)} %copy.15.routes_ref, ...), custom_call_target="tpu_custom_call" | custom-call | tf_op jit(solution)/shard_map/pallas_call | solution.py:187
  481.8 0.0 copy-start.4
  481.8 0.0 copy-start
  481.8 4.8 all-to-all-start
  486.6 0.0 copy-done.4
  486.6 0.1 constant_dynamic-slice_fusion.weight_ref
  486.7 0.0 copy-done
  486.8 0.0 copy-start.2
  486.8 3.4 copy-done.2
  490.1 0.0 copy-start.3
  490.1 7.5 %shard_map.103 = (f32[320,1024]{1,0:T(8,128)S(1)}, bf16[1,4096,1024]{2,1,0:T(8,128)(2,1)}) custom-call(bf16[4,320,1024]{2,1,0:T(8,128)(2,1)S(1)} %bitcast.3, bf16[8,512,1024]{2,1,0:T(8,128)(2,1)S(1)} %copy-done.2), custom_call_target="tpu_custom_call" | custom-call | flops 2684354560 | bytes 16777216 | tf_op jit(solution)/shard_map/pallas_call | solution.py:353
  497.6 0.0 copy-start.1
  497.6 3.4 copy-done.1
  501.0 7.8 %shard_map.104 = (bf16[320,1024]{1,0:T(8,128)(2,1)S(1)}, bf16[1,4096,1024]{2,1,0:T(8,128)(2,1)}) custom-call(bf16[4,320,1024]{2,1,0:T(8,128)(2,1)S(1)} %bitcast.4, bf16[8,512,1024]{2,1,0:T(8,128)(2,1)S(1)} %copy-done.1, f32[320,1024]{1,0:T(8,128)S(1)} %get-tuple-element.21.gate_ref), custom_call_target="tpu_custom_call" | custom-call | flops 2684354560 | bytes 16777216 | tf_op jit(solution)/shard_map/pallas_call | solution.py:353
  508.8 0.0 copy-done.3
  508.8 5.2 shard_map.105
  514.0 68.9 %shard_map.106 = bf16[40,512]{1,0:T(8,128)(2,1)S(1)} custom-call(bf16[2,4,4,40,512]{4,3,2,1,0:T(8,128)(2,1)S(1)} %get-tuple-element.25.part_ref), custom_call_target="tpu_custom_call" | custom-call | tf_op jit(solution)/shard_map/pallas_call | solution.py:289
  583.0 0.0 all-to-all-done.w_ref
  583.0 7.9 %shard_map.107 = (bf16[2,4,4,40,512]{4,3,2,1,0:T(8,128)(2,1)S(1)}, bf16[1,4096,1024]{2,1,0:T(8,128)(2,1)}) custom-call(bf16[320,1024]{1,0:T(8,128)(2,1)S(1)} %get-tuple-element.22.hidden_ref, f32[320,1]{1,0:T(8,128)S(1)} %constant_dynamic-slice_fusion.weight_ref, bf16[8,256,1024]{2,1,0:T(8,128)(2,1)} %all-to-all-done.w_ref, ...), custom_call_target="tpu_custom_call", output_to_operand_aliasing={{1}: (3, {})} | custom-call | flops 1342177280 | bytes 11010048 | tf_op jit(solution)/shard_map/pallas_call | solution.py:404
  590.9 19.2 %shard_map.108 = bf16[40,512]{1,0:T(8,128)(2,1)S(1)} custom-call(bf16[2,4,4,40,512]{4,3,2,1,0:T(8,128)(2,1)S(1)} %get-tuple-element.28.part_ref), custom_call_target="tpu_custom_call" | custom-call | tf_op jit(solution)/shard_map/pallas_call | solution.py:289
  610.1 0.1 pad_maximum_fusion
  610.3 0.1 copy.18
  610.3 0.7 reshape.27
  (2 shorter events, 0.0 us)
Async XLA Ops:
  481.8 4.9 copy-start.4
  481.8 5.0 copy-start
  481.8 101.2 %all-to-all-start = ((bf16[8,256,1024]{2,1,0:T(8,128)(2,1)}), bf16[8,256,1024]{2,1,0:T(8,128)(2,1)}, u32[]{:S(2)}, u32[]{:S(2)}) async-start(bf16[8,256,1024]{2,1,0:T(8,128)(2,1)} %get-tuple-element.26), calls=%async_computation | async-start | bytes 8388608 | tf_op jit(solution)/shard_map/all_to_all | solution.py:432
  486.8 3.4 copy-start.2
  490.1 18.7 %copy-start.3 = (bf16[8,256,1024]{2,1,0:T(8,128)(2,1)S(1)}, bf16[8,256,1024]{2,1,0:T(8,128)(2,1)}, u32[]{:S(2)}) copy-start(bf16[8,256,1024]{2,1,0:T(8,128)(2,1)} %get-tuple-element.24.w_ref) | copy-start | bytes 12582916
  497.6 3.4 copy-start.1

commit v3 on v2

--- a/solution.py
+++ b/solution.py
@@ -14,7 +14,7 @@
 
 
 def exchange_kernel(
-    fs_count, tp_count, experts, pieces,
+    fs_count, tp_count, experts,
     tok_ref, routes_ref, logits_ref, gain_ref, gate_hbm, up_hbm, down_hbm,
     rows_out, weights_out, gate_out, up_out, down_out, rest_out,
     xcol, wown, stage, gate_send, up_send, down_send, rest_send,
@@ -26,7 +26,7 @@
     own = tok_ref.shape[0]
     width, block = stage.shape[1], stage.shape[2]
     part = xcol.shape[2]
-    rows = width // pieces
+    rows = down_send.shape[1]
     barrier = pltpu.get_barrier_semaphore()
     for s in range(1, fs_count):
         pl.semaphore_signal(
@@ -38,7 +38,8 @@
         )
 
     def target(step):
-        return lax.rem(me + fs_count // 2 + step, fs_count)
+        ahead = 1 - 2 * (2 * me // fs_count)
+        return lax.rem(me + fs_count + ahead * (1 + step), fs_count)
 
     def load(hbm, step, slot):
         dst = target(step)
@@ -53,11 +54,11 @@
     scale = lax.rsqrt(jnp.mean(tok * tok, axis=1, keepdims=True) + 1e-05)
     cols = tok_ref[:, pl.ds(pl.multiple_of(my_tp * part, part), part)].astype(jnp.float32)
     xcol[me] = (cols * scale).astype(jnp.bfloat16)
-    first, second = logits_ref[:, 0:1], logits_ref[:, 1:2]
-    lanes = lax.broadcasted_iota(jnp.int32, (own, 128), 1)
+    first, second = logits_ref[0:1, :], logits_ref[1:2, :]
+    ids = lax.broadcasted_iota(jnp.int32, wown.shape, 0)
     wown[...] = jnp.where(
-        routes_ref[:, 0:1] == lanes, 1.0 / (1.0 + jnp.exp(second - first)), 0.0
-    ) + jnp.where(routes_ref[:, 1:2] == lanes, 1.0 / (1.0 + jnp.exp(first - second)), 0.0)
+        routes_ref[0:1, :] == ids, 1.0 / (1.0 + jnp.exp(second - first)), 0.0
+    ) + jnp.where(routes_ref[1:2, :] == ids, 1.0 / (1.0 + jnp.exp(first - second)), 0.0)
     pl.semaphore_wait(barrier, fs_count + tp_count - 2)
 
     def x_copy(dst, sem):
@@ -119,7 +120,7 @@
                 held[dst] = (stage[slot] * gain_ref[...]).astype(jnp.bfloat16)
             else:
                 held[dst] = stage[slot, :rows].astype(jnp.bfloat16)
-                if pieces > 1:
+                if rows < width:
                     rest_send[dst] = stage[slot, rows:].astype(jnp.bfloat16)
 
             @pl.when(dst == me)
@@ -147,7 +148,7 @@
                 t_copies.append(copy)
             x_keep = pltpu.make_async_copy(xcol, rows_out.at[my_tp], own_sem.at[1])
             x_keep.start()
-    if pieces > 1:
+    if rows < width:
         rest_copy = pltpu.make_async_copy(rest_send, rest_out, rest_sem)
         rest_copy.start()
         rest_copy.wait()
@@ -175,35 +176,36 @@
         lax.fori_loop(1, fs_count, finish, 0)
 
 
-def exchange(tokens, routes, logits, gain, gate, up, down, fs_count, tp_count, pieces):
+def exchange(tokens, routes, logits, gain, gate, up, down, fs_count, tp_count, rows):
     experts, width, columns = gate.shape
     block = columns // (fs_count // experts)
-    rows = width // pieces
+    left = width - rows if rows < width else width
+    lines = -(-experts // 8) * 8
     own, model = tokens.shape
     part = model // tp_count
     bf16, dma = jnp.bfloat16, pltpu.SemaphoreType.DMA
     vmem = pl.BlockSpec(memory_space=pltpu.VMEM)
     anywhere = pl.BlockSpec(memory_space=pl.ANY)
     return pl.pallas_call(
-        functools.partial(exchange_kernel, fs_count, tp_count, experts, pieces),
+        functools.partial(exchange_kernel, fs_count, tp_count, experts),
         in_specs=[vmem] * 4 + [anywhere] * 3,
         out_specs=[anywhere] * 6,
         out_shape=[
             jax.ShapeDtypeStruct((tp_count, fs_count, own, part), bf16),
-            jax.ShapeDtypeStruct((fs_count, own, 128), jnp.float32),
+            jax.ShapeDtypeStruct((fs_count, lines, own), jnp.float32),
             jax.ShapeDtypeStruct((fs_count, width, block), bf16),
             jax.ShapeDtypeStruct((fs_count, width, block), bf16),
             jax.ShapeDtypeStruct((fs_count, rows, block), bf16),
-            jax.ShapeDtypeStruct((fs_count, rows, block), bf16),
+            jax.ShapeDtypeStruct((fs_count, left, block), bf16),
         ],
         scratch_shapes=[
             pltpu.VMEM((fs_count, own, part), bf16),
-            pltpu.VMEM((own, 128), jnp.float32),
+            pltpu.VMEM((lines, own), jnp.float32),
             pltpu.VMEM((2, width, block), jnp.float32),
             pltpu.VMEM((fs_count, width, block), bf16),
             pltpu.VMEM((fs_count, width, block), bf16),
             pltpu.VMEM((fs_count, rows, block), bf16),
-            pltpu.VMEM((fs_count, rows, block), bf16),
+            pltpu.VMEM((fs_count, left, block), bf16),
             dma((2,)), dma((3, fs_count)), dma((3, fs_count)), dma((3,)),
             dma((fs_count,)), dma((fs_count,)), dma((fs_count,)), dma((fs_count,)),
             dma((tp_count,)), dma((tp_count,)), dma((2,)), dma,
@@ -282,7 +284,7 @@
         copy2(s).wait_send()
 
 
-def reduce(part, fs_count, tp_count):
+def reduce(part, fs_count, tp_count, number):
     spread, _, experts, own, columns = part.shape
     group = spread * tp_count
     bf16, dma = jnp.bfloat16, pltpu.SemaphoreType.DMA
@@ -298,7 +300,7 @@
             dma((group,)), dma((group,)), dma((experts,)), dma((experts,)), dma,
         ],
         compiler_params=pltpu.CompilerParams(
-            collective_id=1, has_side_effects=True, vmem_limit_bytes=48 * 1024 * 1024
+            collective_id=number, has_side_effects=True, vmem_limit_bytes=48 * 1024 * 1024
         ),
     )(part)
 
@@ -374,7 +376,7 @@
 
 def down_kernel(hidden_ref, weight_ref, w_ref, *rest):
     part_ref, copy_ref = rest[-2:]
-    copy_ref[...] = w_ref[...]
+    copy_ref[:, : w_ref.shape[1]] = w_ref[...]
     part = lax.dot_general(
         hidden_ref[...], w_ref[0], (((1,), (1,)), ((), ())), preferred_element_type=jnp.float32
     )
@@ -385,7 +387,7 @@
         part_ref[h, 0] = blocks[:, h]
 
 
-def project_back(hidden, weight, local, so_far, piece, pieces, experts, spread, tp_count):
+def project_back(hidden, weight, local, so_far, full, experts, spread, tp_count):
     count, width, block = local.shape
     tokens = hidden.shape[0]
     per_tp = count // tp_count
@@ -397,10 +399,15 @@
     ]
     operands = [hidden, weight, local]
     aliases = {}
+    target_spec = pl.BlockSpec((1, full, block), lambda g: (0, g, 0))
     if so_far is not None:
         in_specs.append(pl.BlockSpec(memory_space=pl.ANY))
         operands.append(so_far)
         aliases = {3: 1}
+        per_full = full // width
+        target_spec = pl.BlockSpec(
+            (1, width, block), lambda g: (0, g * per_full + per_full - 1, 0)
+        )
     return pl.pallas_call(
         down_kernel,
         grid=(count,),
@@ -410,13 +417,13 @@
                 (spread, 1, experts, own, width),
                 lambda g: (0, g // per_tp, 0, 0, g % per_tp),
             ),
-            pl.BlockSpec((1, width, block), lambda g: (0, g * pieces + piece, 0)),
+            target_spec,
         ],
         out_shape=[
             jax.ShapeDtypeStruct(
                 (spread, tp_count, experts, own, per_tp * width), jnp.bfloat16
             ),
-            jax.ShapeDtypeStruct((1, count * width * pieces, block), jnp.bfloat16),
+            jax.ShapeDtypeStruct((1, count * full, block), jnp.bfloat16),
         ],
         input_output_aliases=aliases,
         compiler_params=pltpu.CompilerParams(vmem_limit_bytes=VMEM_LIMIT),
@@ -438,26 +445,26 @@
     spread = fs_count // experts
     own, model = tokens.shape
     part_width = model // tp_count
-    pieces = 2 if width % 256 == 0 else 1
+    sent_rows = width - width // 4 if width % 512 == 0 else width
     rows, weights, gate_local, up_local, down_local, rest = exchange(
-        tokens, routes, route_logits, norm_gain[:, None],
-        gate_weight, up_weight, down_weight, fs_count, tp_count, pieces,
+        tokens, routes.T, route_logits.T, norm_gain[:, None],
+        gate_weight, up_weight, down_weight, fs_count, tp_count, sent_rows,
     )
     rows = rows.reshape(tp_count, fs_count * own, part_width)
     mine = lax.axis_index("fs") // spread
-    weight = lax.dynamic_slice_in_dim(weights.reshape(fs_count * own, -1), mine, 1, 1)
+    weight = lax.dynamic_slice_in_dim(weights, mine, 1, 1).reshape(fs_count * own, 1)
     locals_ = [down_local]
-    if pieces > 1:
+    if sent_rows < width:
         locals_.append(swap(rest))
     gate_act, gate_out = project(rows, gate_local)
     hidden, up_out = project(rows, up_local, gate_act)
     down_out, sums = None, []
-    for p in range(pieces):
+    for number, local in enumerate(locals_, 1):
         part, down_out = project_back(
-            hidden, weight, locals_[p], down_out, p, pieces, experts, spread, tp_count
-        )
-        summed = reduce(part, fs_count, tp_count)
-        sums.append(summed.reshape(own, part_width // width, 1, width // pieces))
+            hidden, weight, local, down_out, width, experts, spread, tp_count
+        )
+        summed = reduce(part, fs_count, tp_count, number)
+        sums.append(summed.reshape(own, part_width // width, local.shape[1]))
     mixed = jnp.concatenate(sums, axis=2).reshape(own, part_width)
     return (mixed, gate_out, up_out, down_out)
 

time: 613 us -> 617 us (level)
  Pallas kernels: 593 us -> 601 us
    pallas_call x1, Pallas kernels: 477 us -> 526 us  [exchange(): pl.pallas_call(functools.partial(exchange_kernel, fs_count, tp_count, exp...]
    pallas_call x2, Pallas kernels: 88.1 us -> 48.8 us  [reduce(): pl.pallas_call(functools.partial(reduce_kernel, fs_count, tp_count, exper...]
  transfers between devices with their start and end apart: 1 -> 1, of which waited for: 0 -> 0; matrix products, arithmetic and copies ran while one was open for 0% -> 0% of each run, Pallas kernels for 15% -> 8%
where the time goes in v3:
time: 617 us
  Pallas kernels  601 us (97%)
  local copies, waits for them, and re-layouts  11 us (2%)
    pallas_call x1, Pallas kernels, exchange(): pl.pallas_call(functools.partial(exchange_kernel, fs_count, tp_count, exp...  526 us
    pallas_call x2, Pallas kernels, reduce(): pl.pallas_call(functools.partial(reduce_kernel, fs_count, tp_count, exper...  48.8 us
    pallas_call x2, Pallas kernels, project(): pl.pallas_call(kernel, grid=(count,), in_specs=in_specs, out_specs=[pl.Bl...  15.3 us
  transfers between devices with their start and end apart: 1, of which 0 were waited for; matrix products, arithmetic and copies ran while one was open for 0% of the time, Pallas kernels for 8%

profile of v3, /device:TPU:0, one launch (start us, length us, event | category | flops | bytes accessed | tf_op | source)
XLA Modules:
  0.0 616.6 jit_solution(3438234620866251782)
XLA Ops:
  0.6 1.5 copy.12.gain_ref
  2.2 525.6 %shard_map.102 = (bf16[4,8,40,1024]{3,2,1,0:T(8,128)(2,1)}, f32[8,8,40]{2,1,0:T(8,128)}, bf16[8,512,1024]{2,1,0:T(8,128)(2,1)}, bf16[8,512,1024]{2,1,0:T(8,128)(...) custom-call(bf16[40,4096]{1,0:T(8,128)(2,1)} %tok_ref.1, s32[2,40]{1,0:T(2,128)} %bitcast.11, ...), custom_call_target="tpu_custom_call" | custom-call | tf_op jit(solution)/shard_map/pallas_call | solution.py:189
  527.8 3.6 all-to-all-start
  531.4 0.8 dynamic-slice_reduce_fusion
  532.2 0.1 reshape.28.weight_ref
  532.3 0.0 copy-start
  532.3 1.7 copy-done
  534.0 0.0 copy-start.2
  534.0 3.4 copy-done.2
  537.4 0.0 copy-start.1
  537.4 7.5 %shard_map.103 = (f32[320,1024]{1,0:T(8,128)S(1)}, bf16[1,4096,1024]{2,1,0:T(8,128)(2,1)}) custom-call(bf16[4,320,1024]{2,1,0:T(8,128)(2,1)S(1)} %bitcast.6, bf16[8,512,1024]{2,1,0:T(8,128)(2,1)S(1)} %copy-done.2), custom_call_target="tpu_custom_call" | custom-call | flops 2684354560 | bytes 16777216 | tf_op jit(solution)/shard_map/pallas_call | solution.py:355
  544.9 0.0 copy-done.1
  544.9 7.8 %shard_map.104 = (bf16[320,1024]{1,0:T(8,128)(2,1)S(1)}, bf16[1,4096,1024]{2,1,0:T(8,128)(2,1)}) custom-call(bf16[4,320,1024]{2,1,0:T(8,128)(2,1)S(1)} %bitcast.7, bf16[8,512,1024]{2,1,0:T(8,128)(2,1)S(1)} %copy-done.1, f32[320,1024]{1,0:T(8,128)S(1)} %get-tuple-element.21.gate_ref), custom_call_target="tpu_custom_call" | custom-call | flops 2684354560 | bytes 16777216 | tf_op jit(solution)/shard_map/pallas_call | solution.py:355
  552.7 0.0 copy-start.3
  552.7 2.8 copy-done.3
  555.5 6.8 %shard_map.105 = (bf16[2,4,4,40,768]{4,3,2,1,0:T(8,128)(2,1)S(1)}, bf16[1,4096,1024]{2,1,0:T(8,128)(2,1)}) custom-call(bf16[320,1024]{1,0:T(8,128)(2,1)S(1)} %get-tuple-element.22.hidden_ref, f32[320,1]{1,0:T(8,128)S(1)} %reshape.28.weight_ref, bf16[8,384,1024]{2,1,0:T(8,128)(2,1)S(1)} %copy-done.3), custom_call_target="tpu_custom_call" | custom-call | flops 2013265920 | bytes 16515072 | tf_op jit(solution)/shard_map/pallas_call | solution.py:411
  562.3 28.6 %shard_map.106 = bf16[40,768]{1,0:T(8,128)(2,1)S(1)} custom-call(bf16[2,4,4,40,768]{4,3,2,1,0:T(8,128)(2,1)S(1)} %get-tuple-element.25.part_ref), custom_call_target="tpu_custom_call" | custom-call | tf_op jit(solution)/shard_map/pallas_call | solution.py:291
  590.9 0.0 all-to-all-done.w_ref
  591.0 4.7 shard_map.107
  595.7 20.2 %shard_map.108 = bf16[40,256]{1,0:T(8,128)(2,1)S(1)} custom-call(bf16[2,4,4,40,256]{4,3,2,1,0:T(8,128)(2,1)S(1)} %get-tuple-element.28.part_ref), custom_call_target="tpu_custom_call" | custom-call | tf_op jit(solution)/shard_map/pallas_call | solution.py:291
  615.8 0.1 pad_maximum_fusion
  615.9 0.6 copy.15
  (2 shorter events, 0.0 us)
Async XLA Ops:
  527.8 63.2 %all-to-all-start = ((bf16[8,128,1024]{2,1,0:T(8,128)(2,1)}), bf16[8,128,1024]{2,1,0:T(8,128)(2,1)S(1)}, u32[]{:S(2)}, u32[]{:S(2)}) async-start(bf16[8,128,1024]{2,1,0:T(8,128)(2,1)} %get-tuple-element.26), calls=%async_computation | async-start | bytes 4194304 | tf_op jit(solution)/shard_map/all_to_all | solution.py:439
  532.3 1.7 copy-start
  534.0 3.4 copy-start.2
  537.4 7.5 %copy-start.1 = (bf16[8,512,1024]{2,1,0:T(8,128)(2,1)S(1)}, bf16[8,512,1024]{2,1,0:T(8,128)(2,1)}, u32[]{:S(2)}) copy-start(bf16[8,512,1024]{2,1,0:T(8,128)(2,1)} %get-tuple-element.19.w_ref) | copy-start | bytes 25165828
  552.7 2.8 copy-start.3
